TPU v7x, 32 devices: a whole 2x2x4 slice. The times are simulated.
32 devices in a mesh: ep: 8 (over z, y), tp: 4 (over x, core).
Axes of the slice: x: 2, y: 2, z: 4, core: 2. Of those that a mesh axis runs over, the one named last changes fastest.
Arguments:
- queries: bfloat16 [4096, 2048], P('ep', 'tp'), may hold values from -6 to 6
- forget_pre: float32 [4096, 2048], P('ep', 'tp'), may hold values from -8 to 20
- value_in: bfloat16 [4096, 2048], P('ep', 'tp'), may hold values from -6 to 6
- out_gate: bfloat16 [4096, 2048], P('ep', 'tp'), may hold values from -6 to 6
- lower_bound: float32 [2048], P('tp'), may hold values from 0.5 to 0.8
- out_gain: float32 [128], replicated, may hold values from 0.1 to 1.9
- out_weight: bfloat16 [2048, 2048], P('tp'), may hold values from -0.125 to 0.125
- moe_tokens: bfloat16 [2048, 2048], P('ep'), may hold values from -6 to 6
- moe_gain: float32 [2048], replicated, may hold values from 0.1 to 1.9
- expert_ids: int32 [2048, 4], P('ep'), may hold values from 0 to 15, all different within a row; in each aligned block of 64 rows (0 to 63, 64 to 127, ...) at most 32 rows name the same one
- route_weights: float32 [2048, 4], P('ep'), may hold values from 0.1 to 1
- w_gate: bfloat16 [16, 2048, 1024], P('ep', None, 'tp'), may hold values from -0.125 to 0.125
- w_up: bfloat16 [16, 2048, 1024], P('ep', None, 'tp'), may hold values from -0.125 to 0.125
- w_down: bfloat16 [16, 1024, 2048], P('ep', 'tp'), may hold values from -0.1875 to 0.1875
Outputs:
- mixer_out: bfloat16 [4096, 2048], P(('ep', 'tp'))
- expert_out: bfloat16 [2048, 2048], P(('ep', 'tp'))
Inputs may be any that keep to these rules, and one draw needn't show every extreme that they name: `expert_ids`: each row names 4 different experts. In each aligned block of 64 rows no expert is named by more than 32 rows, and in some block some expert is named by exactly 32 rows.
All inputs are finite; a program needn't handle non-finite values.
Results may differ from a plain program's by a relative error of at most 0.01065.
Values may be sent and summed in bfloat16 or wider, within the bound.
A program may use at most 128 MiB of HBM per device.

v0:
```python
import jax
import jax.numpy as jnp
from jax import lax
from jax.experimental import pallas as pl
from jax.experimental.pallas import tpu as pltpu
from jax.sharding import PartitionSpec as P

HEAD_DIM = 128
BLOCK = 64


EPS = 1e-06
HIGHEST = lax.Precision.HIGHEST


def rms_scale(values, gain):
    return values * lax.rsqrt(jnp.mean(values * values, axis=-1, keepdims=True) + EPS) * gain


def slot_ranks(ids_block, expert_count):
    onehot = (
        ids_block[:, :, None] == jnp.arange(expert_count, dtype=jnp.int32)[None, None, :]
    ).astype(jnp.int32)
    return jnp.sum(onehot * (jnp.cumsum(onehot, axis=1) - 1), axis=2)


MESH = pl.DeviceIdType.MESH
VMEM = pl.BlockSpec(memory_space=pltpu.VMEM)


def ring_place(index, planes):
    plane, side = index // 2, index % 2
    return (1 - side) * plane + side * (2 * planes - 1 - plane)


def ring_index(place, planes):
    back = place // planes
    return (1 - back) * 2 * place + back * ((2 * planes - 1 - place) * 2 + 1)


def ring_setup(count):
    planes = count // 2
    index = lax.axis_index("ep")
    lane = lax.axis_index("tp")
    place = ring_place(index, planes)
    right = ring_index((place + 1) % count, planes)
    left = ring_index((place + count - 1) % count, planes)
    core = lane % 2
    partner = lane + 1 - 2 * core
    return index, lane, core, (right, lane), (left, lane), (index, partner)


def greet(devices):
    barrier = pltpu.get_barrier_semaphore()
    for device in devices:
        pl.semaphore_signal(barrier, inc=1, device_id=device, device_id_type=MESH)
    pl.semaphore_wait(barrier, len(devices))


def remote(source, target, send, receive, device):
    return pltpu.make_async_remote_copy(
        src_ref=source,
        dst_ref=target,
        send_sem=send,
        recv_sem=receive,
        device_id=device,
        device_id_type=MESH,
    )


def gather_kernel(
    count, experts, width, own_ref, gate_ref, up_ref, down_ref, out_ref, held, send, recv, psend, precv
):
    index, lane, core, right, left, partner = ring_setup(count)
    local_experts = gate_ref.shape[0]
    half = held.shape[2]
    turns = count // 2
    greet((right, left, partner))

    def part(side, turn):
        if turn < turns:
            return pl.ds(0, half)
        return pl.ds(side * (half // 2), half // 2)

    def slot(side, turn):
        return turn if side == 0 else count - turn

    def hop(side, turn):
        rows = part(side, turn)
        target = held.at[slot(side, turn), core, rows]
        source = (
            own_ref.at[core, rows] if turn == 1 else held.at[slot(side, turn - 1), core, rows]
        )
        return remote(
            source, target, send.at[side, turn - 1], recv.at[side, turn - 1], (right, left)[side]
        )

    def across(side, turn):
        piece = held.at[slot(side, turn), core, part(side, turn)]
        return remote(piece, piece, psend.at[side, turn - 1], precv.at[side, turn - 1], partner)

    def landed(side, turn):
        piece = held.at[slot(side, turn), 1 - core, part(side, turn)]
        return remote(piece, piece, psend.at[side, turn - 1], precv.at[side, turn - 1], partner)

    def experts_of(block, place):
        rows = block.shape[0]
        tokens = block[:, :width]
        extra = block[:, width:].astype(jnp.float32)
        column = lax.broadcasted_iota(jnp.int32, extra.shape, 1)
        hidden = []
        for expert in range(local_experts):
            number = index * local_experts + expert
            chosen = (column == number) | (column == number + experts)
            weight = jnp.sum(jnp.where(chosen, extra, 0.0), axis=1, keepdims=True)
            gate = jnp.dot(tokens, gate_ref[expert], preferred_element_type=jnp.float32)
            up = jnp.dot(tokens, up_ref[expert], preferred_element_type=jnp.float32)
            hidden.append((jax.nn.silu(gate) * up * weight).astype(jnp.bfloat16))
        total = jnp.dot(hidden[0], down_ref[0], preferred_element_type=jnp.float32)
        for expert in range(1, local_experts):
            total += jnp.dot(
                hidden[expert], down_ref[expert], preferred_element_type=jnp.float32
            )
        for part_at in range(2):
            out_ref[place, part_at] = total[part_at * half : (part_at + 1) * half].astype(
                jnp.bfloat16
            )

    for side in range(2):
        hop(side, 1).start()
    experts_of(own_ref[...].reshape(2 * half, own_ref.shape[2]), 0)
    for turn in range(1, turns + 1):
        for side in range(2):
            hop(side, turn).wait_recv()
            if turn < turns:
                hop(side, turn + 1).start()
            across(side, turn).start()
        for side in range(2):
            landed(side, turn).wait_recv()
        if turn < turns:

            def body(step, carry):
                place = turn + step * (count - 2 * turn)
                experts_of(held[place].reshape(2 * half, held.shape[3]), place)
                return carry

            lax.fori_loop(0, 2, body, 0)
        else:
            experts_of(held[turn].reshape(2 * half, held.shape[3]), turn)
    for turn in range(1, turns + 1):
        for side in range(2):
            hop(side, turn).wait_send()
            across(side, turn).wait_send()


def scatter_kernel(
    count, part_ref, out_ref, total, other, came, final, crossed, send, recv, psend, precv, xsend, xrecv
):
    index, lane, core, right, left, partner = ring_setup(count)
    half = part_ref.shape[2]
    turns = count // 2
    cross_at = lane // 2
    cross = (index, lane + 2 - 4 * cross_at)
    greet((right, left, partner, cross))
    order = [turns]
    for distance in range(turns - 1, 0, -1):
        order += [count - distance, distance]
    order += [0]

    def swap(place):
        return remote(
            part_ref.at[place, 1 - core], other.at[place], psend.at[place], precv.at[place], partner
        )

    for place in order:
        swap(place).start()

    def settle(place):
        swap(place).wait_recv()
        total[place] = (
            part_ref[place, core].astype(jnp.float32) + other[place].astype(jnp.float32)
        ).astype(jnp.bfloat16)

    def rows_of(side, turn):
        if turn > 1:
            return pl.ds(0, half)
        return pl.ds(side * (half // 2), half // 2)

    def hop(side, turn):
        distance = turns - turn + 1
        place = count - distance if side == 0 else distance
        rows = rows_of(side, turn)
        return remote(
            total.at[place, rows],
            came.at[side, turn - 1, rows],
            send.at[side, turn - 1],
            recv.at[side, turn - 1],
            (right, left)[side],
        )

    settle(turns)
    for side in range(2):
        hop(side, 1).start()
    for turn in range(1, turns):
        distance = turns - turn
        for side in range(2):
            settle(count - distance if side == 0 else distance)
        for side in range(2):
            place = count - distance if side == 0 else distance
            rows = rows_of(side, turn)
            hop(side, turn).wait_recv()
            total[place, rows] = (
                total[place, rows].astype(jnp.float32)
                + came[side, turn - 1, rows].astype(jnp.float32)
            ).astype(jnp.bfloat16)
            hop(side, turn + 1).start()
    swap(0).wait_recv()
    for side in range(2):
        hop(side, turns).wait_recv()
    summed = (
        part_ref[0, core].astype(jnp.float32)
        + other[0].astype(jnp.float32)
        + came[0, turns - 1].astype(jnp.float32)
        + came[1, turns - 1].astype(jnp.float32)
    )
    final[...] = summed.astype(jnp.bfloat16).reshape(final.shape)
    over = remote(final.at[1 - cross_at], crossed, xsend, xrecv, cross)
    over.start()
    over.wait_recv()
    out_ref[...] = (final[cross_at].astype(jnp.float32) + crossed[...].astype(jnp.float32)).astype(
        jnp.bfloat16
    )
    over.wait_send()
    for place in range(count):
        swap(place).wait_send()
    for turn in range(1, turns + 1):
        for side in range(2):
            hop(side, turn).wait_send()


def contract(left, right, left_dim, right_dim):
    return lax.dot_general(
        left,
        right,
        (((left_dim,), (right_dim,)), ((), ())),
        precision=HIGHEST,
        preferred_element_type=jnp.float32,
    )


def decay_blocks(forget, bound):
    weight = (1.0 - bound) * jax.nn.sigmoid(-forget)
    logs = jnp.log1p(-weight)
    lower = (
        lax.broadcasted_iota(jnp.int32, (BLOCK, BLOCK), 0)
        >= lax.broadcasted_iota(jnp.int32, (BLOCK, BLOCK), 1)
    )
    ones = jnp.where(lower, 1.0, 0.0)
    blocks = []
    for low in range(0, forget.shape[0], BLOCK):
        cumulative = contract(ones, logs[low : low + BLOCK], 1, 0)
        total = cumulative[BLOCK - 1 :]
        blocks.append((weight[low : low + BLOCK], cumulative, total))
    return lower, blocks


def state_kernel(forget_ref, value_ref, bound_ref, out_ref):
    _, blocks = decay_blocks(forget_ref[...], bound_ref[...])
    memory, span = None, None
    for at, (weight, cumulative, total) in enumerate(blocks):
        values = value_ref[at * BLOCK : (at + 1) * BLOCK].astype(jnp.float32)
        added = contract(values, weight * jnp.exp(total - cumulative), 0, 0)
        memory = added if memory is None else memory * jnp.exp(total) + added
        span = total if span is None else span + total
    decay = jnp.broadcast_to(jnp.exp(span), (16, HEAD_DIM))
    high = decay.astype(jnp.bfloat16).astype(jnp.float32)
    first = lax.broadcasted_iota(jnp.int32, decay.shape, 0) < 8
    out_ref[0, :HEAD_DIM] = memory.astype(jnp.bfloat16)
    out_ref[0, HEAD_DIM:] = jnp.where(first, high, decay - high).astype(jnp.bfloat16)


def mixer_kernel(
    states_ref, query_ref, forget_ref, value_ref, gate_ref, bound_ref, gain_ref, out_ref
):
    def one(hop, memory):
        tail = states_ref[hop, 0, HEAD_DIM:].astype(jnp.float32)
        return memory * (tail[0:1] + tail[8:9]) + states_ref[hop, 0, :HEAD_DIM].astype(jnp.float32)

    memory = lax.fori_loop(
        0, lax.axis_index("ep"), one, jnp.zeros((HEAD_DIM, HEAD_DIM), jnp.float32)
    )
    lower, blocks = decay_blocks(forget_ref[...], bound_ref[...])
    for at, (weight, cumulative, total) in enumerate(blocks):
        rows = slice(at * BLOCK, (at + 1) * BLOCK)
        values = value_ref[rows].astype(jnp.float32)
        decayed_query = query_ref[rows].astype(jnp.float32) * jnp.exp(cumulative)
        scores = contract(decayed_query, weight * jnp.exp(-cumulative), 1, 1)
        result = contract(jnp.where(lower, scores, 0.0), values, 1, 0)
        result += contract(decayed_query, memory, 1, 1)
        added = contract(values, weight * jnp.exp(total - cumulative), 0, 0)
        memory = memory * jnp.exp(total) + added
        gate = jax.nn.silu(gate_ref[rows].astype(jnp.float32))
        out_ref[rows] = (rms_scale(result, gain_ref[...]) * gate).astype(jnp.bfloat16)


def head_block(rows):
    return pl.BlockSpec((rows, HEAD_DIM), lambda head: (0, head))


def head_states(forget_pre, value_in, lower_bound):
    rows, width = forget_pre.shape
    heads = width // HEAD_DIM
    return pl.pallas_call(
        state_kernel,
        grid=(heads,),
        out_shape=jax.ShapeDtypeStruct((heads, HEAD_DIM + 16, HEAD_DIM), jnp.bfloat16),
        in_specs=[head_block(rows), head_block(rows), head_block(1)],
        out_specs=pl.BlockSpec((1, HEAD_DIM + 16, HEAD_DIM), lambda head: (head, 0, 0)),
        cost_estimate=pl.CostEstimate(
            flops=10**9, bytes_accessed=8 * forget_pre.size, transcendentals=0
        ),
        name="head_states",
    )(forget_pre, value_in, lower_bound[None])


def mix_heads(states, queries, forget_pre, value_in, out_gate, lower_bound, out_gain):
    rows, width = forget_pre.shape
    heads = width // HEAD_DIM
    count = states.shape[0]
    return pl.pallas_call(
        mixer_kernel,
        grid=(heads,),
        out_shape=jax.ShapeDtypeStruct((rows, width), jnp.bfloat16),
        in_specs=[
            pl.BlockSpec((count, 1, HEAD_DIM + 16, HEAD_DIM), lambda head: (0, head, 0, 0)),
            head_block(rows),
            head_block(rows),
            head_block(rows),
            head_block(rows),
            head_block(1),
            pl.BlockSpec((1, HEAD_DIM), lambda head: (0, 0)),
        ],
        out_specs=head_block(rows),
        cost_estimate=pl.CostEstimate(
            flops=4 * 10**9, bytes_accessed=16 * forget_pre.size, transcendentals=0
        ),
        name="mix_heads",
    )(states, queries, forget_pre, value_in, out_gate, lower_bound[None], out_gain[None])


def prepare_kernel(experts, token_ref, gain_ref, ids_ref, weights_ref, out_ref):
    rows, width = token_ref.shape
    normed = rms_scale(token_ref[...].astype(jnp.float32), gain_ref[...]).astype(jnp.bfloat16)
    margin = out_ref.shape[2] - width
    column = lax.broadcasted_iota(jnp.int32, (rows, margin), 1)
    extra = jnp.zeros((rows, margin), jnp.float32)
    for choice in range(ids_ref.shape[1]):
        number = ids_ref[:, choice : choice + 1]
        weight = weights_ref[:, choice : choice + 1]
        high = weight.astype(jnp.bfloat16).astype(jnp.float32)
        extra += jnp.where(column == number, high, 0.0)
        extra += jnp.where(column == number + experts, weight - high, 0.0)
    extra = extra.astype(jnp.bfloat16)
    step = rows // 4
    for core in range(2):
        for cross in range(2):
            low = (2 * cross + core) * step
            out_ref[core, cross * step : (cross + 1) * step, :width] = normed[low : low + step]
            out_ref[core, cross * step : (cross + 1) * step, width:] = extra[low : low + step]


def prepare(tokens, gain, ids, weights, experts):
    rows, width = tokens.shape
    margin = -(-2 * experts // 128) * 128
    return pl.pallas_call(
        lambda *refs: prepare_kernel(experts, *refs),
        out_shape=jax.ShapeDtypeStruct((2, rows // 2, width + margin), jnp.bfloat16),
        in_specs=[VMEM] * 4,
        out_specs=VMEM,
        cost_estimate=pl.CostEstimate(
            flops=10**6, bytes_accessed=4 * tokens.size, transcendentals=0
        ),
        name="prepare",
    )(tokens, gain[None], ids, weights)


def moe_gather(full, w_gate, w_up, w_down, ep_count, experts):
    half, stride = full.shape[1:]
    width = w_down.shape[2]
    turns = ep_count // 2
    sems = pltpu.SemaphoreType.DMA((2, turns))
    rows = 2 * half * ep_count
    flops = 2 * rows * w_gate.size * 3
    return pl.pallas_call(
        lambda *refs: gather_kernel(ep_count, experts, width, *refs),
        out_shape=jax.ShapeDtypeStruct((ep_count, 2, half, width), jnp.bfloat16),
        in_specs=[VMEM] * 4,
        out_specs=VMEM,
        scratch_shapes=[
            pltpu.VMEM((ep_count, 2, half, stride), jnp.bfloat16),
            sems,
            sems,
            sems,
            sems,
        ],
        compiler_params=pltpu.CompilerParams(
            collective_id=0, has_side_effects=True, vmem_limit_bytes=58 * 2**20
        ),
        cost_estimate=pl.CostEstimate(
            flops=flops, bytes_accessed=100 * 2**20, transcendentals=0
        ),
        name="moe_gather",
    )(full, w_gate, w_up, w_down)


def moe_scatter(parts):
    count, _, half, width = parts.shape
    turns = count // 2
    sems = pltpu.SemaphoreType.DMA((2, turns))
    each = pltpu.SemaphoreType.DMA((count,))
    block = (count, half, width)
    return pl.pallas_call(
        lambda *refs: scatter_kernel(count, *refs),
        out_shape=jax.ShapeDtypeStruct((half // 2, width), jnp.bfloat16),
        in_specs=[VMEM],
        out_specs=VMEM,
        scratch_shapes=[
            pltpu.VMEM(block, jnp.bfloat16),
            pltpu.VMEM(block, jnp.bfloat16),
            pltpu.VMEM((2, turns, half, width), jnp.bfloat16),
            pltpu.VMEM((2, half // 2, width), jnp.bfloat16),
            pltpu.VMEM((half // 2, width), jnp.bfloat16),
            sems,
            sems,
            each,
            each,
            pltpu.SemaphoreType.DMA,
            pltpu.SemaphoreType.DMA,
        ],
        compiler_params=pltpu.CompilerParams(
            collective_id=1, has_side_effects=True, vmem_limit_bytes=58 * 2**20
        ),
        cost_estimate=pl.CostEstimate(
            flops=0, bytes_accessed=150 * 2**20, transcendentals=0
        ),
        name="moe_scatter",
    )(parts)


def sparse_experts(
    moe_tokens, moe_gain, expert_ids, route_weights, w_gate, w_up, w_down, model_width
):
    lanes = lax.axis_size("tp")
    lane_index = lax.axis_index("tp")
    ep_count = lax.axis_size("ep")
    qrows = moe_tokens.shape[0] // lanes
    top_count = expert_ids.shape[1]
    local_experts = w_gate.shape[0]
    expert_count = local_experts * ep_count
    capacity = max(2, 2 * qrows * top_count // expert_count)
    send_tokens = lax.dynamic_slice_in_dim(moe_tokens, lane_index * qrows, qrows, 0)
    send_ids = lax.dynamic_slice_in_dim(expert_ids, lane_index * qrows, qrows, 0)
    quarters = send_tokens.shape[0] // qrows
    normed = rms_scale(send_tokens.astype(jnp.float32), moe_gain).astype(jnp.bfloat16)
    ids_block = send_ids.reshape(quarters, qrows * top_count)
    ranks = slot_ranks(ids_block, expert_count)
    quarter_base = jnp.arange(quarters, dtype=jnp.int32)[:, None] * (expert_count * capacity)
    slot_index = (quarter_base + ids_block * capacity + ranks).reshape(-1)
    source_row = jnp.arange(quarters * qrows * top_count, dtype=jnp.int32) // top_count
    sources = (
        jnp.full((quarters * expert_count * capacity,), quarters * qrows, jnp.int32)
        .at[slot_index]
        .set(source_row)
    )
    padded = jnp.concatenate([normed, jnp.zeros((1, model_width), jnp.bfloat16)], axis=0)
    outgoing = padded[sources].reshape(quarters, ep_count, local_experts * capacity, model_width)
    arrived = lax.all_to_all(outgoing, "ep", split_axis=1, concat_axis=1, tiled=True)
    piece = lax.all_gather(arrived, "tp", axis=0, tiled=True)
    shaped = piece.reshape(piece.shape[0], ep_count, local_experts, capacity, model_width)
    gate_pre = jnp.einsum("qsecd,edf->qsecf", shaped, w_gate, preferred_element_type=jnp.float32)
    up_pre = jnp.einsum("qsecd,edf->qsecf", shaped, w_up, preferred_element_type=jnp.float32)
    hidden = (jax.nn.silu(gate_pre) * up_pre).astype(jnp.bfloat16)
    lane_rows = ep_count * local_experts * capacity
    projected = jnp.einsum("qsecf,efd->qsecd", hidden, w_down, preferred_element_type=jnp.float32)
    expert_sum = lax.psum_scatter(
        projected.reshape(lax.axis_size("tp") * lane_rows, model_width).astype(jnp.bfloat16),
        "tp",
        scatter_dimension=0,
        tiled=True,
    )
    leaving = expert_sum.reshape(ep_count, local_experts * capacity, model_width)
    returned = lax.all_to_all(leaving, "ep", split_axis=0, concat_axis=0, tiled=True)
    returned = returned.reshape(expert_count * capacity, model_width)
    own_quarter = lane_index * (quarters // lanes)
    own_ids = lax.dynamic_index_in_dim(ids_block, own_quarter, 0, keepdims=False)
    own_ranks = lax.dynamic_index_in_dim(ranks, own_quarter, 0, keepdims=False)
    picked = (
        returned[own_ids * capacity + own_ranks]
        .astype(jnp.float32)
        .reshape(qrows, top_count, model_width)
    )
    own_weights = lax.dynamic_slice_in_dim(route_weights, lane_index * qrows, qrows, 0)
    expert_out = jnp.sum(picked * own_weights[:, :, None], axis=1).astype(jnp.bfloat16)
    return expert_out


def local(
    queries,
    forget_pre,
    value_in,
    out_gate,
    lower_bound,
    out_gain,
    out_weight,
    moe_tokens,
    moe_gain,
    expert_ids,
    route_weights,
    w_gate,
    w_up,
    w_down,
):
    lanes = lax.axis_size("tp")
    ep_count = lax.axis_size("ep")
    model_width = out_weight.shape[1]
    packed = head_states(forget_pre, value_in, lower_bound)
    tokens, top_count = expert_ids.shape
    dense_slots = 2 * (tokens // lanes) * top_count * lanes
    dense = lanes == 4 and ep_count % 2 == 0 and tokens * ep_count <= dense_slots
    if dense:
        experts = w_gate.shape[0] * ep_count
        full = prepare(moe_tokens, moe_gain, expert_ids, route_weights, experts)
        full, packed = lax.optimization_barrier((full, packed))
    gathered = lax.all_gather(packed, "ep")
    if dense:
        parts = moe_gather(full, w_gate, w_up, w_down, ep_count, experts)
        gathered, parts = lax.optimization_barrier((gathered, parts))
    gated = mix_heads(
        gathered, queries, forget_pre, value_in, out_gate, lower_bound, out_gain
    )
    mixer_part = jnp.dot(gated, out_weight, preferred_element_type=jnp.float32).astype(
        jnp.bfloat16
    )
    if dense:
        mixer_part, parts = lax.optimization_barrier((mixer_part, parts))
    mixer_sum = lax.psum_scatter(mixer_part, "tp", scatter_dimension=0, tiled=True)
    if dense:
        expert_out = moe_scatter(parts)
    else:
        expert_out = sparse_experts(
            moe_tokens, moe_gain, expert_ids, route_weights, w_gate, w_up, w_down, model_width
        )
    return (mixer_sum, expert_out)


def solution(mesh):
    in_specs = (
        P("ep", "tp"),
        P("ep", "tp"),
        P("ep", "tp"),
        P("ep", "tp"),
        P("tp"),
        P(),
        P("tp", None),
        P("ep", None),
        P(),
        P("ep", None),
        P("ep", None),
        P("ep", None, "tp"),
        P("ep", None, "tp"),
        P("ep", "tp", None),
    )
    out_specs = (P(("ep", "tp"), None), P(("ep", "tp"), None))
    return jax.shard_map(local, mesh=mesh, in_specs=in_specs, out_specs=out_specs, check_vma=False)
```

profile of v0, /device:TPU:0, one launch (start us, length us, event | category | flops | bytes accessed | tf_op | source)
XLA Modules:
  0.0 179.7 jit_solution(1599949037729198133)
XLA Ops:
  7.2 0.0 copy-start
  7.2 0.0 all-gather.3.cloned.1.call-start
  7.2 1.6 copy.18.refs_2_
  8.8 1.5 copy.19.refs_3_
  10.3 5.2 %head_states.1 = bf16[4,144,128]{2,1,0:T(8,128)(2,1)} custom-call(f32[512,512]{1,0:T(8,128)} %forget_ref.3, bf16[512,512]{1,0:T(8,128)(2,1)} %value_ref.3, f32[1,512]{1,0:T(1,128)} %bitcast.8), custom_call_target="tpu_custom_call" | custom-call | flops 1000000000 | bytes 2097152 | tf_op jit(solution)/shard_map/head_states/pallas_call | solution.py:313
  15.5 3.2 %prepare.1.refs_0_ = bf16[2,128,2176]{2,1,0:T(8,128)(2,1)} custom-call(bf16[256,2048]{1,0:T(8,128)(2,1)} %refs_0_.1, f32[1,2048]{1,0:T(1,128)} %bitcast.6, s32[256,4]{1,0:T(8,128)} %copy.18.refs_2_, f32[256,4]{1,0:T(8,128)} %copy.19.refs_3_), custom_call_target="tpu_custom_call" | custom-call | flops 1000000 | bytes 2097152 | tf_op jit(solution)/shard_map/prepare/pallas_call | solution.py:375
  18.7 0.0 all-gather.3.cloned.1.call-update
  18.7 0.0 reduce-scatter.2.cloned.1.call-start
  18.8 72.2 %moe_gather.1.refs_0_ = bf16[8,2,128,2048]{3,2,1,0:T(8,128)(2,1)} custom-call(bf16[2,128,2176]{2,1,0:T(8,128)(2,1)} %prepare.1.refs_0_, bf16[2,2048,256]{2,1,0:T(8,128)(2,1)} %refs_1_.1, bf16[2,2048,256]{2,1,0:T(8,128)(2,1)} %refs_2_.2, bf16[2,256,2048]{2,1,0:T(8,128)(2,1)} %refs_3_.2), custom_call_target="tpu_custom_call" | custom-call | flops 12884901888 | bytes 104857600 | tf_op jit(solution)/shard_map/moe_gather/pallas_call | solution.py:394
  91.0 0.0 all-gather.3.cloned.1.call-done
  91.1 12.7 %mix_heads.1 = bf16[512,512]{1,0:T(8,128)(2,1)} custom-call(bf16[8,4,144,128]{3,2,1,0:T(8,128)(2,1)} %bitcast.7, bf16[512,512]{1,0:T(8,128)(2,1)} %query_ref.1, f32[512,512]{1,0:T(8,128)} %forget_ref.3, bf16[512,512]{1,0:T(8,128)(2,1)} %value_ref.3, bf16[512,512]{1,0:T(8,128)(2,1)} %gate_ref.1, f32[1,512]{1,0:T(1,128)} %bitcast.9, f32[1,128]{1,0:T(1,128)} %bitcast.10), custom_call_target="tpu_custom_call" | custom-call | flops 4000000000 | bytes 4194304 | tf_op jit(solution)/shard_map/mix_heads/pallas_call | solution.py:330
  103.8 0.0 copy-done
  103.8 3.7 %convolution_convert_fusion = bf16[512,2048]{1,0:T(8,128)(2,1)} fusion(bf16[512,512]{1,0:T(8,128)(2,1)} %mix_heads.1, bf16[512,2048]{1,0:T(8,128)(2,1)S(1)} %copy-done), kind=kOutput, calls=%fused_computation | convolution fusion | flops 1074790400 | bytes 4718592 | tf_op jit(solution)/shard_map/dot_general | solution.py:541
  107.4 0.0 reduce-scatter.2.cloned.1.call-update
  107.4 63.7 %moe_scatter.1 = bf16[64,2048]{1,0:T(8,128)(2,1)} custom-call(bf16[8,2,128,2048]{3,2,1,0:T(8,128)(2,1)} %moe_gather.1.refs_0_), custom_call_target="tpu_custom_call" | custom-call | bytes 157286400 | tf_op jit(solution)/shard_map/moe_scatter/pallas_call | solution.py:422
  171.1 0.0 reduce-scatter.2.cloned.1.call-done
  171.1 1.7 copy.21
Async XLA Ops:
  7.2 96.6 %copy-start = (bf16[512,2048]{1,0:T(8,128)(2,1)S(1)}, bf16[512,2048]{1,0:T(8,128)(2,1)}, u32[]{:S(2)}) copy-start(bf16[512,2048]{1,0:T(8,128)(2,1)} %param.20) | copy-start | bytes 6291460
  7.2 83.9 %all-gather.3.cloned.1.call-start = ((), (), s32[]{:S(2)}) async-start(), calls=%async_computation.2 | async-start | bytes 1327104 | tf_op jit(solution)/shard_map/all_gather | solution.py:534
  18.7 152.4 %reduce-scatter.2.cloned.1.call-start = ((), (), s32[]{:S(2)}) async-start(), calls=%async_computation.1 | async-start | bytes 2621440 | tf_op jit(solution)/shard_map/reduce_scatter | solution.py:546
Sparse Core Ops, SparseCore 0:
  18.9 50.6 all-gather.2
  107.6 33.7 reduce-scatter.1
where the time goes:
time: 180 us
  Pallas kernels  157 us (87%)
  between operations  14.1 us (8%)
  local copies, waits for them, and re-layouts  4.78 us (3%)
  matrix products  3.65 us (2%)
    pallas_call x1, Pallas kernels, moe_gather(): pl.pallas_call(lambda *refs: gather_kernel(ep_count, experts, width, *ref...  72.2 us
    pallas_call x1, Pallas kernels, moe_scatter(): pl.pallas_call(lambda *refs: scatter_kernel(count, *refs), out_shape=jax....  63.7 us
    pallas_call x1, Pallas kernels, mix_heads(): pl.pallas_call(mixer_kernel, grid=(heads,), out_shape=jax.ShapeDtypeStruc...  12.7 us
    pallas_call x1, Pallas kernels, head_states(): pl.pallas_call(state_kernel, grid=(heads,), out_shape=jax.ShapeDtypeStruc...  5.19 us
    unnamed x5, local copies, waits for them, and re-layouts  4.78 us
    dot_general x1, matrix products, local(): jnp.dot(gated, out_weight, preferred_element_type=jnp.float32)  3.65 us
  transfers between devices with their start and end apart: 2, of which 0 were waited for; matrix products, arithmetic and copies ran while one was open for 0% of the time, Pallas kernels for 76%

commit v1 on v0

v1 whole, which is shorter than its diff:
```python
import jax
import jax.numpy as jnp
from jax import lax
from jax.experimental import pallas as pl
from jax.experimental.pallas import tpu as pltpu
from jax.sharding import PartitionSpec as P

HEAD_DIM = 128
BLOCK = 64


EPS = 1e-06
HIGHEST = lax.Precision.HIGHEST


def rms_scale(values, gain):
    return values * lax.rsqrt(jnp.mean(values * values, axis=-1, keepdims=True) + EPS) * gain


def slot_ranks(ids_block, expert_count):
    onehot = (
        ids_block[:, :, None] == jnp.arange(expert_count, dtype=jnp.int32)[None, None, :]
    ).astype(jnp.int32)
    return jnp.sum(onehot * (jnp.cumsum(onehot, axis=1) - 1), axis=2)


MESH = pl.DeviceIdType.MESH
VMEM = pl.BlockSpec(memory_space=pltpu.VMEM)


def remote(source, target, send, receive, device):
    return pltpu.make_async_remote_copy(
        src_ref=source,
        dst_ref=target,
        send_sem=send,
        recv_sem=receive,
        device_id=device,
        device_id_type=MESH,
    )


def flip(value):
    return value + 1 - 2 * (value % 2)


def fused_kernel(
    tok_hbm,
    gain_ref,
    ids_ref,
    route_ref,
    wg_hbm,
    wu_hbm,
    wd_hbm,
    query_hbm,
    forget_hbm,
    value_hbm,
    gate_hbm,
    bound_ref,
    ogain_ref,
    ow_hbm,
    mix_out,
    moe_out,
    wg,
    wu,
    wd,
    query,
    forget,
    value,
    ogate,
    ow,
    held,
    part,
    other,
    sums,
    bx,
    by,
    cx,
    cy,
    zr,
    wbuf,
    cum,
    near,
    qdec,
    gated,
    mpart,
    mother,
    msum,
    mx,
    st,
    sz,
    tables,
    columns,
    send,
    recv,
    lsem,
):
    f32, bf16 = jnp.float32, jnp.bfloat16
    ep = lax.axis_index("ep")
    tp = lax.axis_index("tp")
    z, y = ep // 2, ep % 2
    x, c = tp // 2, tp % 2
    planes, _, quarters, piece, width = held.shape
    seq, chans = forget.shape
    heads = chans // HEAD_DIM
    top = ids_ref.shape[0]
    local_experts, _, hidden_units = wg.shape
    xfirst = bx.shape[2]
    xrows, yrows = pl.ds(0, xfirst), pl.ds(xfirst, piece - xfirst)
    fold = piece // 2
    low_half, high_half = pl.ds(0, fold), pl.ds(fold, piece - fold)
    partner = (ep, flip(tp))
    xn = (ep, (tp + 2) % 4)
    yn = (flip(ep), tp)
    others = (z, flip(z), (z + 2) % 4, 3 - z)
    zn = [(others[k] * 2 + y, tp) for k in range(planes)]

    def spot(dx, dc):
        return pl.ds(pl.multiple_of((((x + dx) % 2) * 2 + (c + dc) % 2) * piece, piece), piece)

    own_loads = []
    for dc in range(2):
        for dx in range(2):
            own_loads.append(
                pltpu.make_async_copy(
                    tok_hbm.at[spot(dx, dc)], held.at[0, dc, dx], lsem.at[8 + len(own_loads)]
                )
            )
            own_loads[-1].start()
    loads = {}
    for at, (name, source, target) in enumerate(
        (
            ("forget", forget_hbm, forget),
            ("value", value_hbm, value),
            ("query", query_hbm, query),
            ("wg", wg_hbm, wg),
            ("wu", wu_hbm, wu),
            ("wd", wd_hbm, wd),
            ("gate", gate_hbm, ogate),
            ("ow", ow_hbm, ow),
        )
    ):
        loads[name] = pltpu.make_async_copy(source, target, lsem.at[at])
        loads[name].start()

    peers = [partner, xn, yn] + zn[1:]
    barrier = pltpu.get_barrier_semaphore()
    for device in peers:
        pl.semaphore_signal(barrier, inc=1, device_id=device, device_id_type=MESH)

    copies = {}

    def put(name, source, target, device):
        at = len(copies)
        copies[name] = remote(source, target, send.at[at], recv.at[at], device)
        copies[name].start()

    def got(*names):
        for name in names:
            copies[name].wait_recv()

    def ready(*names):
        for name in names:
            if name in loads:
                loads.pop(name).wait()

    def run_experts(block, table, store):
        ready("wg", "wu", "wd")
        tokens = rms_scale(block.astype(f32), gain_ref[...]).astype(bf16)
        hidden = []
        for expert in range(local_experts):
            chosen = table[:, :top] == (ep * local_experts + expert).astype(f32)
            weight = jnp.sum(
                jnp.where(chosen, table[:, top : 2 * top], 0.0), axis=1, keepdims=True
            )
            gate = jnp.dot(tokens, wg[expert], preferred_element_type=f32)
            up = jnp.dot(tokens, wu[expert], preferred_element_type=f32)
            hidden.append((jax.nn.silu(gate) * up * weight).astype(bf16))
        hidden = jnp.concatenate(hidden, axis=1)
        down = wd[...].reshape(local_experts * hidden_units, width)
        step = min(width, 512)
        for low in range(0, width, step):
            total = jnp.dot(hidden, down[:, low : low + step], preferred_element_type=f32)
            store(low, step, total.astype(bf16))

    def experts_own(dy):
        if dy == 1:
            got("down0", "down1", "ty0")
        else:
            for load in own_loads:
                load.wait()
        columns[0, dy] = jnp.transpose(tables[0, dy])
        table = jnp.concatenate(
            [columns[0, dy, spot(dx, dc)] for dc in range(2) for dx in range(2)], axis=0
        )

        def store(low, step, total):
            part[0, :, 2 * dy : 2 * dy + 2, :, low : low + step] = total.reshape(2, 2, piece, step)

        block = held[0, :, 2 * dy : 2 * dy + 2].reshape(4 * piece, width)
        run_experts(block, table, store)
        if dy == 1:
            put("r10", part.at[0, 1], other.at[0], partner)

    shown = []

    def experts_plane(k, side):
        if side == 1:
            got(*[f"d{q}{k}" for q in range(quarters)])
        if k not in shown:
            shown.append(k)
            got(f"ty{k}")
            for dy in range(2):
                columns[k, dy] = jnp.transpose(tables[k, dy])
        table = jnp.concatenate(
            [columns[k, dy, spot(dx, side)] for dy in range(2) for dx in range(2)], axis=0
        )

        def store(low, step, total):
            part[k, side, :, :, low : low + step] = total.reshape(quarters, piece, step)

        run_experts(held[k, side].reshape(quarters * piece, width), table, store)
        if side == 1:
            put(f"r1{k}", part.at[k, 1], other.at[k], partner)

    def start():
        tables[0, 0, :top] = ids_ref[...].astype(f32)
        tables[0, 0, top : 2 * top] = route_ref[...]
        pl.semaphore_wait(barrier, len(peers))
        for load in own_loads[:2]:
            load.wait()
        del own_loads[:2]
        put("z1", held.at[0, 0, 0], held.at[1, 0, 0], zn[1])
        put("own0", held.at[0, 0, 0], held.at[0, 0, 2], yn)
        put("own1", held.at[0, 0, 1], held.at[0, 0, 3], yn)
        for k in range(1, planes):
            put(f"tz{k}", tables.at[0, 0], tables.at[k, 0], zn[k])
        put("ty0", tables.at[0, 0], tables.at[0, 1], yn)

    def far(k):
        put(f"z{k}", held.at[0, 0, 0], held.at[k, 0, 0], zn[k])

    def own():
        for dx in range(2):
            got(f"own{dx}")
            put(f"down{dx}", held.at[0, 0, 2 + dx], held.at[0, 1, 2 + dx], partner)

    def plane(k):
        got(f"z{k}")
        mine = held.at[k, 0, 0]
        put(f"x{k}", mine, held.at[k, 0, 1], xn)
        put(f"y{k}", mine, held.at[k, 0, 2], yn)
        put(f"d0{k}", mine, held.at[k, 1, 0], partner)
        got(f"tz{k}")
        put(f"ty{k}", tables.at[k, 0], tables.at[k, 1], yn)

    def from_x(k):
        got(f"x{k}")
        put(f"fy{k}", held.at[k, 0, 1, low_half], held.at[k, 0, 3, low_half], yn)
        put(f"d1{k}", held.at[k, 0, 1], held.at[k, 1, 1], partner)

    def from_y(k):
        got(f"y{k}")
        put(f"fx{k}", held.at[k, 0, 2, high_half], held.at[k, 0, 3, high_half], xn)
        put(f"d2{k}", held.at[k, 0, 2], held.at[k, 1, 2], partner)

    def corner(k):
        got(f"fy{k}", f"fx{k}")
        put(f"d3{k}", held.at[k, 0, 3], held.at[k, 1, 3], partner)

    def add(*terms):
        total = terms[0].astype(f32)
        for term in terms[1:]:
            total = total + term.astype(f32)
        return total.astype(bf16)

    def rs_first(k):
        got(f"r1{k}")

        def body(q, carry):
            sums[k, q % 2, q // 2] = add(part[k, 0, q], other[k, q])
            return carry

        lax.fori_loop(0, quarters, body, 0)
        put(f"r2x{k}", sums.at[k, 1, :, xrows], bx.at[k], xn)
        put(f"r2y{k}", sums.at[k, :, 1, yrows], by.at[k], yn)

    def rs_x(k):
        got(f"r2x{k}")
        for dy in (1, 0):
            sums[k, 0, dy, :xfirst] = add(sums[k, 0, dy, :xfirst], bx[k, dy])
            if dy == 1:
                put(f"r3y{k}", sums.at[k, 0, 1, xrows], cy.at[k], yn)

    def rs_y(k):
        got(f"r2y{k}")
        for dx in (1, 0):
            sums[k, dx, 0, xfirst:] = add(sums[k, dx, 0, xfirst:], by[k, dx])
            if dx == 1:
                put(f"r3x{k}", sums.at[k, 1, 0, yrows], cx.at[k], xn)

    def rs_third(k):
        got(f"r3y{k}", f"r3x{k}")
        sums[k, 0, 0, :xfirst] = add(sums[k, 0, 0, :xfirst], cy[k])
        sums[k, 0, 0, xfirst:] = add(sums[k, 0, 0, xfirst:], cx[k])
        if k > 0:
            put(f"r4{k}", sums.at[k, 0, 0], zr.at[k - 1], zn[k])

    def rs_end():
        got(*[f"r4{k}" for k in range(1, planes)])
        moe_out[...] = add(sums[0, 0, 0], *[zr[k] for k in range(planes - 1)])

    def mix_decay():
        ready("forget")
        tile = min(seq, 256)
        row = lax.broadcasted_iota(jnp.int32, (tile, tile), 0)
        col = lax.broadcasted_iota(jnp.int32, (tile, tile), 1)
        ones = jnp.where((row >= col) & (row // BLOCK == col // BLOCK), 1.0, 0.0).astype(bf16)
        for low in range(0, seq, tile):
            weight = (1.0 - bound_ref[...]) * jax.nn.sigmoid(-forget[low : low + tile])
            logs = jnp.log1p(-weight)
            high = logs.astype(bf16)
            rest = (logs - high.astype(f32)).astype(bf16)
            wbuf[low : low + tile] = weight
            cum[low : low + tile] = jnp.dot(ones, high, preferred_element_type=f32) + jnp.dot(
                ones, rest, preferred_element_type=f32
            )

    def dot_of(left, right, left_dim, right_dim):
        return lax.dot_general(
            left, right, (((left_dim,), (right_dim,)), ((), ())), preferred_element_type=f32
        )

    def mix_local(first, last):
        ready("value", "query")
        lower = lax.broadcasted_iota(jnp.int32, (BLOCK, BLOCK), 0) >= lax.broadcasted_iota(
            jnp.int32, (BLOCK, BLOCK), 1
        )

        def body(head, carry):
            lanes = pl.ds(pl.multiple_of(head * HEAD_DIM, HEAD_DIM), HEAD_DIM)
            memory, before = None, None
            for low in range(0, seq, BLOCK):
                rows = pl.ds(low, BLOCK)
                cumulative = cum[rows, lanes]
                total = jnp.exp(cumulative[BLOCK - 1 :])
                values = value[rows, lanes]
                raised = wbuf[rows, lanes] * jnp.exp(-cumulative)
                decayed = query[rows, lanes].astype(f32) * jnp.exp(cumulative)
                decayed_low = decayed.astype(bf16)
                scores = dot_of(decayed_low, raised.astype(bf16), 1, 1)
                scores = jnp.where(lower, scores, 0.0).astype(bf16)
                result = dot_of(scores, values, 1, 0)
                added = dot_of(values, (raised * total).astype(bf16), 0, 0)
                if memory is None:
                    qdec[rows, lanes] = decayed_low
                    memory, before = added, total
                else:
                    result += dot_of(decayed_low, memory.astype(bf16), 1, 1)
                    qdec[rows, lanes] = (decayed * before).astype(bf16)
                    memory, before = memory * total + added, before * total
                near[rows, lanes] = result
            store_state(st.at[0, head], memory, before)
            return carry

        lax.fori_loop(first, last, body, 0)

    def store_state(target, memory, decay):
        decay = jnp.broadcast_to(decay, (16, HEAD_DIM))
        high = decay.astype(bf16).astype(f32)
        top = lax.broadcasted_iota(jnp.int32, decay.shape, 0) < 8
        target[:HEAD_DIM] = memory.astype(bf16)
        target[HEAD_DIM:] = jnp.where(top, high, decay - high).astype(bf16)

    def load_state(source):
        tail = source[HEAD_DIM:].astype(f32)
        return source[:HEAD_DIM].astype(f32), tail[0:1] + tail[8:9]

    upper = y.astype(f32)

    def state_plane():
        put("sy", st.at[0], st.at[1], yn)

    def state_combine():
        got("sy")

        def body(head, carry):
            mine, mine_decay = load_state(st.at[0, head])
            theirs, theirs_decay = load_state(st.at[1, head])
            early = mine + upper * (theirs - mine)
            late = theirs + upper * (mine - theirs)
            late_decay = theirs_decay + upper * (mine_decay - theirs_decay)
            store_state(sz.at[0, head], early * late_decay + late, mine_decay * theirs_decay)
            return carry

        lax.fori_loop(0, heads, body, 0)
        for k in range(1, planes):
            put(f"sz{k}", sz.at[0], sz.at[k], zn[k])

    def mix_finish():
        got(*[f"sz{k}" for k in range(1, planes)])
        ready("gate")

        def body(head, carry):
            lanes = pl.ds(pl.multiple_of(head * HEAD_DIM, HEAD_DIM), HEAD_DIM)
            memory = jnp.zeros((HEAD_DIM, HEAD_DIM), f32)
            for place in range(planes - 1):
                keep = jnp.where(z > place, 1.0, 0.0)
                state, decay = load_state(sz.at[others[place], head])
                memory = memory * (decay * keep + (1.0 - keep)) + state * keep
            state, decay = load_state(st.at[1, head])
            memory = memory * (decay * upper + (1.0 - upper)) + state * upper
            result = near[:, lanes] + dot_of(qdec[:, lanes], memory.astype(bf16), 1, 1)
            gate = jax.nn.silu(ogate[:, lanes].astype(f32))
            gated[:, lanes] = (rms_scale(result, ogain_ref[...]) * gate).astype(bf16)
            return carry

        lax.fori_loop(0, heads, body, 0)

    def mix_project():
        ready("ow")
        lanes, rows = mpart.shape[:2]
        step = min(width, 512)
        for low in range(0, width, step):
            total = jnp.dot(gated[...], ow[:, low : low + step], preferred_element_type=f32)
            mpart[:, :, low : low + step] = total.astype(bf16).reshape(lanes, rows, step)
        for dx in (1, 0):
            there = (x + dx) % 2
            put(f"m1{dx}", mpart.at[2 * there + 1 - c], mother.at[dx], partner)

    def mix_cross():
        got("m11")
        msum[...] = add(mpart[2 * (1 - x) + c], mother[1])
        put("m2", msum, mx, xn)

    def mix_end():
        got("m10", "m2")
        mix_out[...] = add(mpart[2 * x + c], mother[0], mx[...])

    start()
    far(3)
    plane(1)
    mix_decay()
    plane(3)
    experts_own(0)
    far(2)
    mix_local(0, heads // 2)
    from_y(1)
    from_x(3)
    from_y(3)
    plane(2)
    from_x(1)
    mix_local(heads // 2, heads)
    corner(3)
    own()
    state_plane()
    experts_plane(3, 0)
    experts_plane(3, 1)
    from_y(2)
    corner(1)
    from_x(2)
    rs_first(3)
    experts_plane(1, 1)
    state_combine()
    experts_plane(1, 0)
    rs_first(1)
    corner(2)
    experts_plane(2, 0)
    experts_plane(2, 1)
    rs_y(3)
    rs_x(3)
    experts_own(1)
    rs_x(1)
    rs_first(2)
    rs_third(3)
    rs_y(1)
    rs_x(2)
    rs_first(0)
    rs_third(1)
    mix_finish()
    mix_project()
    rs_y(2)
    rs_x(0)
    mix_cross()
    rs_third(2)
    rs_y(0)
    mix_end()
    rs_third(0)
    rs_end()
    for copy in copies.values():
        copy.wait_send()


def hand_over(mixed, routed, mix_out, moe_out):
    mix_out[...] = mixed[...]
    moe_out[...] = routed[...]


def fused(
    queries,
    forget_pre,
    value_in,
    out_gate,
    lower_bound,
    out_gain,
    out_weight,
    moe_tokens,
    moe_gain,
    expert_ids,
    route_weights,
    w_gate,
    w_up,
    w_down,
    planes,
    lanes,
):
    bf16, f32 = jnp.bfloat16, jnp.float32
    seq, chans = queries.shape
    heads = chans // HEAD_DIM
    rows, width = moe_tokens.shape
    piece = rows // lanes
    top = expert_ids.shape[1]
    xfirst = piece // 2
    slot = (piece, width)
    vmem, dma = pltpu.VMEM, pltpu.SemaphoreType.DMA
    count = 80
    flops = 2 * rows * planes * 2 * w_gate.size * 3
    anywhere = pl.BlockSpec(memory_space=pl.ANY)
    mixed, routed = pl.pallas_call(
        fused_kernel,
        out_shape=(
            jax.ShapeDtypeStruct((seq // lanes, width), bf16),
            jax.ShapeDtypeStruct(slot, bf16),
        ),
        in_specs=[
            anywhere, VMEM, VMEM, VMEM, anywhere, anywhere, anywhere,
            anywhere, anywhere, anywhere, anywhere, VMEM, VMEM, anywhere,
        ],
        out_specs=(VMEM, VMEM),
        scratch_shapes=[
            vmem(w_gate.shape, bf16),
            vmem(w_up.shape, bf16),
            vmem(w_down.shape, bf16),
            vmem((seq, chans), bf16),
            vmem((seq, chans), f32),
            vmem((seq, chans), bf16),
            vmem((seq, chans), bf16),
            vmem((chans, width), bf16),
            vmem((planes, 2, 4, piece, width), bf16),
            vmem((planes, 2, 4, piece, width), bf16),
            vmem((planes, 4, piece, width), bf16),
            vmem((planes, 2, 2, piece, width), bf16),
            vmem((planes, 2, xfirst, width), bf16),
            vmem((planes, 2, piece - xfirst, width), bf16),
            vmem((planes, piece - xfirst, width), bf16),
            vmem((planes, xfirst, width), bf16),
            vmem((planes - 1, piece, width), bf16),
            vmem((seq, chans), f32),
            vmem((seq, chans), f32),
            vmem((seq, chans), f32),
            vmem((seq, chans), bf16),
            vmem((seq, chans), bf16),
            vmem((lanes, seq // lanes, width), bf16),
            vmem((2, seq // lanes, width), bf16),
            vmem((seq // lanes, width), bf16),
            vmem((seq // lanes, width), bf16),
            vmem((2, heads, HEAD_DIM + 16, HEAD_DIM), bf16),
            vmem((planes, heads, HEAD_DIM + 16, HEAD_DIM), bf16),
            vmem((planes, 2, 2 * top, rows), f32),
            vmem((planes, 2, rows, 2 * top), f32),
            dma((count,)),
            dma((count,)),
            dma((12,)),
        ],
        compiler_params=pltpu.CompilerParams(
            collective_id=0, has_side_effects=True, vmem_limit_bytes=63 * 2**20
        ),
        cost_estimate=pl.CostEstimate(
            flops=flops, bytes_accessed=100 * 2**20, transcendentals=0
        ),
        name="fused",
    )(
        moe_tokens,
        moe_gain[None],
        expert_ids.T,
        route_weights.T,
        w_gate,
        w_up,
        w_down,
        queries,
        forget_pre,
        value_in,
        out_gate,
        lower_bound[None],
        out_gain[None],
        out_weight,
    )
    return pl.pallas_call(
        hand_over,
        out_shape=tuple(jax.ShapeDtypeStruct(a.shape, a.dtype) for a in (mixed, routed)),
        in_specs=[VMEM, VMEM],
        out_specs=(VMEM, VMEM),
        name="hand_over",
    )(mixed, routed)


def contract(left, right, left_dim, right_dim):
    return lax.dot_general(
        left,
        right,
        (((left_dim,), (right_dim,)), ((), ())),
        precision=HIGHEST,
        preferred_element_type=jnp.float32,
    )


def decay_blocks(forget, bound):
    weight = (1.0 - bound) * jax.nn.sigmoid(-forget)
    logs = jnp.log1p(-weight)
    lower = (
        lax.broadcasted_iota(jnp.int32, (BLOCK, BLOCK), 0)
        >= lax.broadcasted_iota(jnp.int32, (BLOCK, BLOCK), 1)
    )
    ones = jnp.where(lower, 1.0, 0.0)
    blocks = []
    for low in range(0, forget.shape[0], BLOCK):
        cumulative = contract(ones, logs[low : low + BLOCK], 1, 0)
        total = cumulative[BLOCK - 1 :]
        blocks.append((weight[low : low + BLOCK], cumulative, total))
    return lower, blocks


def state_kernel(forget_ref, value_ref, bound_ref, out_ref):
    _, blocks = decay_blocks(forget_ref[...], bound_ref[...])
    memory, span = None, None
    for at, (weight, cumulative, total) in enumerate(blocks):
        values = value_ref[at * BLOCK : (at + 1) * BLOCK].astype(jnp.float32)
        added = contract(values, weight * jnp.exp(total - cumulative), 0, 0)
        memory = added if memory is None else memory * jnp.exp(total) + added
        span = total if span is None else span + total
    decay = jnp.broadcast_to(jnp.exp(span), (16, HEAD_DIM))
    high = decay.astype(jnp.bfloat16).astype(jnp.float32)
    first = lax.broadcasted_iota(jnp.int32, decay.shape, 0) < 8
    out_ref[0, :HEAD_DIM] = memory.astype(jnp.bfloat16)
    out_ref[0, HEAD_DIM:] = jnp.where(first, high, decay - high).astype(jnp.bfloat16)


def mixer_kernel(
    states_ref, query_ref, forget_ref, value_ref, gate_ref, bound_ref, gain_ref, out_ref
):
    def one(hop, memory):
        tail = states_ref[hop, 0, HEAD_DIM:].astype(jnp.float32)
        return memory * (tail[0:1] + tail[8:9]) + states_ref[hop, 0, :HEAD_DIM].astype(jnp.float32)

    memory = lax.fori_loop(
        0, lax.axis_index("ep"), one, jnp.zeros((HEAD_DIM, HEAD_DIM), jnp.float32)
    )
    lower, blocks = decay_blocks(forget_ref[...], bound_ref[...])
    for at, (weight, cumulative, total) in enumerate(blocks):
        rows = slice(at * BLOCK, (at + 1) * BLOCK)
        values = value_ref[rows].astype(jnp.float32)
        decayed_query = query_ref[rows].astype(jnp.float32) * jnp.exp(cumulative)
        scores = contract(decayed_query, weight * jnp.exp(-cumulative), 1, 1)
        result = contract(jnp.where(lower, scores, 0.0), values, 1, 0)
        result += contract(decayed_query, memory, 1, 1)
        added = contract(values, weight * jnp.exp(total - cumulative), 0, 0)
        memory = memory * jnp.exp(total) + added
        gate = jax.nn.silu(gate_ref[rows].astype(jnp.float32))
        out_ref[rows] = (rms_scale(result, gain_ref[...]) * gate).astype(jnp.bfloat16)


def head_block(rows):
    return pl.BlockSpec((rows, HEAD_DIM), lambda head: (0, head))


def head_states(forget_pre, value_in, lower_bound):
    rows, width = forget_pre.shape
    heads = width // HEAD_DIM
    return pl.pallas_call(
        state_kernel,
        grid=(heads,),
        out_shape=jax.ShapeDtypeStruct((heads, HEAD_DIM + 16, HEAD_DIM), jnp.bfloat16),
        in_specs=[head_block(rows), head_block(rows), head_block(1)],
        out_specs=pl.BlockSpec((1, HEAD_DIM + 16, HEAD_DIM), lambda head: (head, 0, 0)),
        cost_estimate=pl.CostEstimate(
            flops=10**9, bytes_accessed=8 * forget_pre.size, transcendentals=0
        ),
        name="head_states",
    )(forget_pre, value_in, lower_bound[None])


def mix_heads(states, queries, forget_pre, value_in, out_gate, lower_bound, out_gain):
    rows, width = forget_pre.shape
    heads = width // HEAD_DIM
    count = states.shape[0]
    return pl.pallas_call(
        mixer_kernel,
        grid=(heads,),
        out_shape=jax.ShapeDtypeStruct((rows, width), jnp.bfloat16),
        in_specs=[
            pl.BlockSpec((count, 1, HEAD_DIM + 16, HEAD_DIM), lambda head: (0, head, 0, 0)),
            head_block(rows),
            head_block(rows),
            head_block(rows),
            head_block(rows),
            head_block(1),
            pl.BlockSpec((1, HEAD_DIM), lambda head: (0, 0)),
        ],
        out_specs=head_block(rows),
        cost_estimate=pl.CostEstimate(
            flops=4 * 10**9, bytes_accessed=16 * forget_pre.size, transcendentals=0
        ),
        name="mix_heads",
    )(states, queries, forget_pre, value_in, out_gate, lower_bound[None], out_gain[None])


def sparse_experts(
    moe_tokens, moe_gain, expert_ids, route_weights, w_gate, w_up, w_down, model_width
):
    lanes = lax.axis_size("tp")
    lane_index = lax.axis_index("tp")
    ep_count = lax.axis_size("ep")
    qrows = moe_tokens.shape[0] // lanes
    top_count = expert_ids.shape[1]
    local_experts = w_gate.shape[0]
    expert_count = local_experts * ep_count
    capacity = max(2, 2 * qrows * top_count // expert_count)
    send_tokens = lax.dynamic_slice_in_dim(moe_tokens, lane_index * qrows, qrows, 0)
    send_ids = lax.dynamic_slice_in_dim(expert_ids, lane_index * qrows, qrows, 0)
    quarters = send_tokens.shape[0] // qrows
    normed = rms_scale(send_tokens.astype(jnp.float32), moe_gain).astype(jnp.bfloat16)
    ids_block = send_ids.reshape(quarters, qrows * top_count)
    ranks = slot_ranks(ids_block, expert_count)
    quarter_base = jnp.arange(quarters, dtype=jnp.int32)[:, None] * (expert_count * capacity)
    slot_index = (quarter_base + ids_block * capacity + ranks).reshape(-1)
    source_row = jnp.arange(quarters * qrows * top_count, dtype=jnp.int32) // top_count
    sources = (
        jnp.full((quarters * expert_count * capacity,), quarters * qrows, jnp.int32)
        .at[slot_index]
        .set(source_row)
    )
    padded = jnp.concatenate([normed, jnp.zeros((1, model_width), jnp.bfloat16)], axis=0)
    outgoing = padded[sources].reshape(quarters, ep_count, local_experts * capacity, model_width)
    arrived = lax.all_to_all(outgoing, "ep", split_axis=1, concat_axis=1, tiled=True)
    piece = lax.all_gather(arrived, "tp", axis=0, tiled=True)
    shaped = piece.reshape(piece.shape[0], ep_count, local_experts, capacity, model_width)
    gate_pre = jnp.einsum("qsecd,edf->qsecf", shaped, w_gate, preferred_element_type=jnp.float32)
    up_pre = jnp.einsum("qsecd,edf->qsecf", shaped, w_up, preferred_element_type=jnp.float32)
    hidden = (jax.nn.silu(gate_pre) * up_pre).astype(jnp.bfloat16)
    lane_rows = ep_count * local_experts * capacity
    projected = jnp.einsum("qsecf,efd->qsecd", hidden, w_down, preferred_element_type=jnp.float32)
    expert_sum = lax.psum_scatter(
        projected.reshape(lax.axis_size("tp") * lane_rows, model_width).astype(jnp.bfloat16),
        "tp",
        scatter_dimension=0,
        tiled=True,
    )
    leaving = expert_sum.reshape(ep_count, local_experts * capacity, model_width)
    returned = lax.all_to_all(leaving, "ep", split_axis=0, concat_axis=0, tiled=True)
    returned = returned.reshape(expert_count * capacity, model_width)
    own_quarter = lane_index * (quarters // lanes)
    own_ids = lax.dynamic_index_in_dim(ids_block, own_quarter, 0, keepdims=False)
    own_ranks = lax.dynamic_index_in_dim(ranks, own_quarter, 0, keepdims=False)
    picked = (
        returned[own_ids * capacity + own_ranks]
        .astype(jnp.float32)
        .reshape(qrows, top_count, model_width)
    )
    own_weights = lax.dynamic_slice_in_dim(route_weights, lane_index * qrows, qrows, 0)
    expert_out = jnp.sum(picked * own_weights[:, :, None], axis=1).astype(jnp.bfloat16)
    return expert_out


def local(
    queries,
    forget_pre,
    value_in,
    out_gate,
    lower_bound,
    out_gain,
    out_weight,
    moe_tokens,
    moe_gain,
    expert_ids,
    route_weights,
    w_gate,
    w_up,
    w_down,
):
    lanes = lax.axis_size("tp")
    ep_count = lax.axis_size("ep")
    model_width = out_weight.shape[1]
    tokens, top_count = expert_ids.shape
    dense_slots = 2 * (tokens // lanes) * top_count * lanes
    if lanes == 4 and ep_count == 8 and tokens * ep_count <= dense_slots:
        return fused(
            queries,
            forget_pre,
            value_in,
            out_gate,
            lower_bound,
            out_gain,
            out_weight,
            moe_tokens,
            moe_gain,
            expert_ids,
            route_weights,
            w_gate,
            w_up,
            w_down,
            ep_count // 2,
            lanes,
        )
    packed = head_states(forget_pre, value_in, lower_bound)
    gathered = lax.all_gather(packed, "ep")
    gated = mix_heads(
        gathered, queries, forget_pre, value_in, out_gate, lower_bound, out_gain
    )
    mixer_part = jnp.dot(gated, out_weight, preferred_element_type=jnp.float32).astype(
        jnp.bfloat16
    )
    mixer_sum = lax.psum_scatter(mixer_part, "tp", scatter_dimension=0, tiled=True)
    expert_out = sparse_experts(
        moe_tokens, moe_gain, expert_ids, route_weights, w_gate, w_up, w_down, model_width
    )
    return (mixer_sum, expert_out)


def solution(mesh):
    in_specs = (
        P("ep", "tp"),
        P("ep", "tp"),
        P("ep", "tp"),
        P("ep", "tp"),
        P("tp"),
        P(),
        P("tp", None),
        P("ep", None),
        P(),
        P("ep", None),
        P("ep", None),
        P("ep", None, "tp"),
        P("ep", None, "tp"),
        P("ep", "tp", None),
    )
    out_specs = (P(("ep", "tp"), None), P(("ep", "tp"), None))
    return jax.shard_map(local, mesh=mesh, in_specs=in_specs, out_specs=out_specs, check_vma=False)
```

time: 180 us -> 96.4 us (0.54)
  Pallas kernels: 157 us -> 95.6 us
  between operations: 14.1 us -> 0.64 us
  local copies, waits for them, and re-layouts: 4.78 us -> 0 us
  matrix products: 3.65 us -> 0 us
    pallas_call x5 -> x2, Pallas kernels: 157 us -> 95.6 us  [the longest x1 93.6 us: fused(): pl.pallas_call(fused_kernel, out_shape=(jax.ShapeDtypeStruct((seq // lane...]
    unnamed x5 -> x0, local copies, waits for them, and re-layouts: 4.78 us -> none
    dot_general x1 -> x0, matrix products: 3.65 us -> none  [local(): jnp.dot(gated, out_weight, preferred_element_type=jnp.float32)]
  transfers between devices with their start and end apart: 2 -> 0, of which waited for: 0 -> 0; matrix products, arithmetic and copies ran while one was open for 0% -> 0% of each run, Pallas kernels for 76% -> 0%
where the time goes in v1:
time: 96.4 us; the launch traced here: 96.2 us
  Pallas kernels  95.6 us (99%)
    pallas_call x1, Pallas kernels, fused(): pl.pallas_call(fused_kernel, out_shape=(jax.ShapeDtypeStruct((seq // lane...  93.6 us
    pallas_call x1, Pallas kernels, fused(): pl.pallas_call(hand_over, out_shape=tuple((jax.ShapeDtypeStruct(a.shape,...  2.02 us

profile of v1, /device:TPU:0, one launch (start us, length us, event | category | flops | bytes accessed | tf_op | source)
XLA Modules:
  0.0 96.2 jit_solution(15277381733574133825)
XLA Ops:
  0.6 93.6 %fused.1 = (bf16[128,2048]{1,0:T(8,128)(2,1)}, bf16[64,2048]{1,0:T(8,128)(2,1)}) custom-call(bf16[256,2048]{1,0:T(8,128)(2,1)} %tok_hbm.1, f32[1,2048]{1,0:T(1,128)} %bitcast.5, s32[4,256]{1,0:T(4,128)} %bitcast.6, f32[4,256]{1,0:T(4,128)} %bitcast.7, bf16[2,2048,256]{2,1,0:T(8,128)(2,1)} %wg_hbm.1, bf16[2,2048,256]{2,1,0:T(8,128)(2,1)} %wu_hbm.1, ...), custom_call_target="tpu_custom_call" | custom-call | flops 12884901888 | bytes 104857600 | tf_op jit(solution)/shard_map/fused/pallas_call | solution.py:528
  94.2 2.0 %hand_over.1 = (bf16[128,2048]{1,0:T(8,128)(2,1)}, bf16[64,2048]{1,0:T(8,128)(2,1)}) custom-call(bf16[128,2048]{1,0:T(8,128)(2,1)} %get-tuple-element.4.mixed, bf16[64,2048]{1,0:T(8,128)(2,1)} %get-tuple-element.5.routed), custom_call_target="tpu_custom_call" | custom-call | tf_op jit(solution)/shard_map/hand_over/pallas_call | solution.py:597

commit v2 on v1

--- a/solution.py
+++ b/solution.py
@@ -10,6 +10,7 @@
 
 
 EPS = 1e-06
+X_SHARE = (2, 4, 4, 4)
 HIGHEST = lax.Precision.HIGHEST
 
 
@@ -45,9 +46,9 @@
 
 def fused_kernel(
     tok_hbm,
-    gain_ref,
-    ids_ref,
-    route_ref,
+    gain_hbm,
+    ids_hbm,
+    route_hbm,
     wg_hbm,
     wu_hbm,
     wd_hbm,
@@ -55,11 +56,16 @@
     forget_hbm,
     value_hbm,
     gate_hbm,
-    bound_ref,
-    ogain_ref,
+    bound_hbm,
+    ogain_hbm,
     ow_hbm,
     mix_out,
     moe_out,
+    gain_ref,
+    ids_ref,
+    route_ref,
+    bound_ref,
+    ogain_ref,
     wg,
     wu,
     wd,
@@ -102,10 +108,10 @@
     planes, _, quarters, piece, width = held.shape
     seq, chans = forget.shape
     heads = chans // HEAD_DIM
-    top = ids_ref.shape[0]
+    top = ids_hbm.shape[0]
     local_experts, _, hidden_units = wg.shape
-    xfirst = bx.shape[2]
-    xrows, yrows = pl.ds(0, xfirst), pl.ds(xfirst, piece - xfirst)
+    xfirst = [piece * share // 8 for share in X_SHARE]
+    ysize = [piece - rows for rows in xfirst]
     fold = piece // 2
     low_half, high_half = pl.ds(0, fold), pl.ds(fold, piece - fold)
     partner = (ep, flip(tp))
@@ -114,6 +120,11 @@
     others = (z, flip(z), (z + 2) % 4, 3 - z)
     zn = [(others[k] * 2 + y, tp) for k in range(planes)]
 
+    peers = [partner, xn, yn] + zn[1:]
+    barrier = pltpu.get_barrier_semaphore()
+    for device in peers:
+        pl.semaphore_signal(barrier, inc=1, device_id=device, device_id_type=MESH)
+
     def spot(dx, dc):
         return pl.ds(pl.multiple_of((((x + dx) % 2) * 2 + (c + dc) % 2) * piece, piece), piece)
 
@@ -122,31 +133,31 @@
         for dx in range(2):
             own_loads.append(
                 pltpu.make_async_copy(
-                    tok_hbm.at[spot(dx, dc)], held.at[0, dc, dx], lsem.at[8 + len(own_loads)]
+                    tok_hbm.at[spot(dx, dc)], held.at[0, dc, dx], lsem.at[13 + len(own_loads)]
                 )
             )
             own_loads[-1].start()
     loads = {}
     for at, (name, source, target) in enumerate(
         (
+            ("ids", ids_hbm, ids_ref),
+            ("route", route_hbm, route_ref),
+            ("bound", bound_hbm, bound_ref),
             ("forget", forget_hbm, forget),
             ("value", value_hbm, value),
             ("query", query_hbm, query),
+            ("gain", gain_hbm, gain_ref),
             ("wg", wg_hbm, wg),
             ("wu", wu_hbm, wu),
             ("wd", wd_hbm, wd),
             ("gate", gate_hbm, ogate),
+            ("ogain", ogain_hbm, ogain_ref),
             ("ow", ow_hbm, ow),
         )
     ):
         loads[name] = pltpu.make_async_copy(source, target, lsem.at[at])
         loads[name].start()
 
-    peers = [partner, xn, yn] + zn[1:]
-    barrier = pltpu.get_barrier_semaphore()
-    for device in peers:
-        pl.semaphore_signal(barrier, inc=1, device_id=device, device_id_type=MESH)
-
     copies = {}
 
     def put(name, source, target, device):
@@ -164,7 +175,7 @@
                 loads.pop(name).wait()
 
     def run_experts(block, table, store):
-        ready("wg", "wu", "wd")
+        ready("gain", "wg", "wu", "wd")
         tokens = rms_scale(block.astype(f32), gain_ref[...]).astype(bf16)
         hidden = []
         for expert in range(local_experts):
@@ -223,15 +234,16 @@
             put(f"r1{k}", part.at[k, 1], other.at[k], partner)
 
     def start():
-        tables[0, 0, :top] = ids_ref[...].astype(f32)
-        tables[0, 0, top : 2 * top] = route_ref[...]
         pl.semaphore_wait(barrier, len(peers))
         for load in own_loads[:2]:
             load.wait()
         del own_loads[:2]
         put("z1", held.at[0, 0, 0], held.at[1, 0, 0], zn[1])
         put("own0", held.at[0, 0, 0], held.at[0, 0, 2], yn)
-        put("own1", held.at[0, 0, 1], held.at[0, 0, 3], yn)
+        put("own1", held.at[0, 0, 1, low_half], held.at[0, 0, 3, low_half], yn)
+        ready("ids", "route")
+        tables[0, 0, :top] = ids_ref[...].astype(f32)
+        tables[0, 0, top : 2 * top] = route_ref[...]
         for k in range(1, planes):
             put(f"tz{k}", tables.at[0, 0], tables.at[k, 0], zn[k])
         put("ty0", tables.at[0, 0], tables.at[0, 1], yn)
@@ -239,10 +251,13 @@
     def far(k):
         put(f"z{k}", held.at[0, 0, 0], held.at[k, 0, 0], zn[k])
 
-    def own():
-        for dx in range(2):
-            got(f"own{dx}")
-            put(f"down{dx}", held.at[0, 0, 2 + dx], held.at[0, 1, 2 + dx], partner)
+    def own(dx):
+        got(f"own{dx}")
+        if dx == 0:
+            put("ownx", held.at[0, 0, 2, high_half], held.at[0, 0, 3, high_half], xn)
+        else:
+            got("ownx")
+        put(f"down{dx}", held.at[0, 0, 2 + dx], held.at[0, 1, 2 + dx], partner)
 
     def plane(k):
         got(f"z{k}")
@@ -275,33 +290,37 @@
 
     def rs_first(k):
         got(f"r1{k}")
+        xf, ys = xfirst[k], ysize[k]
 
         def body(q, carry):
             sums[k, q % 2, q // 2] = add(part[k, 0, q], other[k, q])
             return carry
 
         lax.fori_loop(0, quarters, body, 0)
-        put(f"r2x{k}", sums.at[k, 1, :, xrows], bx.at[k], xn)
-        put(f"r2y{k}", sums.at[k, :, 1, yrows], by.at[k], yn)
+        put(f"r2x{k}", sums.at[k, 1, :, pl.ds(0, xf)], bx.at[k, :, pl.ds(0, xf)], xn)
+        put(f"r2y{k}", sums.at[k, :, 1, pl.ds(xf, ys)], by.at[k, :, pl.ds(0, ys)], yn)
 
     def rs_x(k):
         got(f"r2x{k}")
+        xf = xfirst[k]
         for dy in (1, 0):
-            sums[k, 0, dy, :xfirst] = add(sums[k, 0, dy, :xfirst], bx[k, dy])
+            sums[k, 0, dy, :xf] = add(sums[k, 0, dy, :xf], bx[k, dy, :xf])
             if dy == 1:
-                put(f"r3y{k}", sums.at[k, 0, 1, xrows], cy.at[k], yn)
+                put(f"r3y{k}", sums.at[k, 0, 1, pl.ds(0, xf)], cy.at[k, pl.ds(0, xf)], yn)
 
     def rs_y(k):
         got(f"r2y{k}")
+        xf, ys = xfirst[k], ysize[k]
         for dx in (1, 0):
-            sums[k, dx, 0, xfirst:] = add(sums[k, dx, 0, xfirst:], by[k, dx])
+            sums[k, dx, 0, xf:] = add(sums[k, dx, 0, xf:], by[k, dx, :ys])
             if dx == 1:
-                put(f"r3x{k}", sums.at[k, 1, 0, yrows], cx.at[k], xn)
+                put(f"r3x{k}", sums.at[k, 1, 0, pl.ds(xf, ys)], cx.at[k, pl.ds(0, ys)], xn)
 
     def rs_third(k):
         got(f"r3y{k}", f"r3x{k}")
-        sums[k, 0, 0, :xfirst] = add(sums[k, 0, 0, :xfirst], cy[k])
-        sums[k, 0, 0, xfirst:] = add(sums[k, 0, 0, xfirst:], cx[k])
+        xf, ys = xfirst[k], ysize[k]
+        sums[k, 0, 0, :xf] = add(sums[k, 0, 0, :xf], cy[k, :xf])
+        sums[k, 0, 0, xf:] = add(sums[k, 0, 0, xf:], cx[k, :ys])
         if k > 0:
             put(f"r4{k}", sums.at[k, 0, 0], zr.at[k - 1], zn[k])
 
@@ -310,7 +329,7 @@
         moe_out[...] = add(sums[0, 0, 0], *[zr[k] for k in range(planes - 1)])
 
     def mix_decay():
-        ready("forget")
+        ready("forget", "bound")
         tile = min(seq, 256)
         row = lax.broadcasted_iota(jnp.int32, (tile, tile), 0)
         col = lax.broadcasted_iota(jnp.int32, (tile, tile), 1)
@@ -398,7 +417,7 @@
 
     def mix_finish():
         got(*[f"sz{k}" for k in range(1, planes)])
-        ready("gate")
+        ready("gate", "ogain")
 
         def body(head, carry):
             lanes = pl.ds(pl.multiple_of(head * HEAD_DIM, HEAD_DIM), HEAD_DIM)
@@ -438,52 +457,53 @@
 
     start()
     far(3)
+    mix_decay()
+    own(0)
+    mix_local(0, heads // 2)
     plane(1)
-    mix_decay()
     plane(3)
     experts_own(0)
     far(2)
-    mix_local(0, heads // 2)
+    from_x(1)
+    from_y(3)
+    from_x(3)
     from_y(1)
-    from_x(3)
-    from_y(3)
     plane(2)
-    from_x(1)
     mix_local(heads // 2, heads)
     corner(3)
-    own()
     state_plane()
     experts_plane(3, 0)
     experts_plane(3, 1)
+    corner(1)
     from_y(2)
-    corner(1)
     from_x(2)
     rs_first(3)
     experts_plane(1, 1)
+    own(1)
     state_combine()
     experts_plane(1, 0)
     rs_first(1)
     corner(2)
-    experts_plane(2, 0)
     experts_plane(2, 1)
     rs_y(3)
     rs_x(3)
+    experts_plane(2, 0)
+    rs_first(2)
+    rs_y(1)
+    rs_x(1)
     experts_own(1)
-    rs_x(1)
-    rs_first(2)
+    mix_finish()
     rs_third(3)
-    rs_y(1)
     rs_x(2)
     rs_first(0)
+    rs_y(2)
+    mix_project()
     rs_third(1)
-    mix_finish()
-    mix_project()
-    rs_y(2)
-    rs_x(0)
     mix_cross()
     rs_third(2)
     rs_y(0)
     mix_end()
+    rs_x(0)
     rs_third(0)
     rs_end()
     for copy in copies.values():
@@ -519,12 +539,13 @@
     rows, width = moe_tokens.shape
     piece = rows // lanes
     top = expert_ids.shape[1]
-    xfirst = piece // 2
+    xmost = max(X_SHARE) * piece // 8
+    ymost = piece - min(X_SHARE) * piece // 8
     slot = (piece, width)
     vmem, dma = pltpu.VMEM, pltpu.SemaphoreType.DMA
     count = 80
     flops = 2 * rows * planes * 2 * w_gate.size * 3
-    anywhere = pl.BlockSpec(memory_space=pl.ANY)
+    anywhere = pl.BlockSpec(memory_space=pltpu.HBM)
     mixed, routed = pl.pallas_call(
         fused_kernel,
         out_shape=(
@@ -532,11 +553,16 @@
             jax.ShapeDtypeStruct(slot, bf16),
         ),
         in_specs=[
-            anywhere, VMEM, VMEM, VMEM, anywhere, anywhere, anywhere,
-            anywhere, anywhere, anywhere, anywhere, VMEM, VMEM, anywhere,
+            anywhere, anywhere, anywhere, anywhere, anywhere, anywhere, anywhere,
+            anywhere, anywhere, anywhere, anywhere, anywhere, anywhere, anywhere,
         ],
         out_specs=(VMEM, VMEM),
         scratch_shapes=[
+            vmem((1, width), f32),
+            vmem((top, rows), jnp.int32),
+            vmem((top, rows), f32),
+            vmem((1, chans), f32),
+            vmem((1, HEAD_DIM), f32),
             vmem(w_gate.shape, bf16),
             vmem(w_up.shape, bf16),
             vmem(w_down.shape, bf16),
@@ -549,10 +575,10 @@
             vmem((planes, 2, 4, piece, width), bf16),
             vmem((planes, 4, piece, width), bf16),
             vmem((planes, 2, 2, piece, width), bf16),
-            vmem((planes, 2, xfirst, width), bf16),
-            vmem((planes, 2, piece - xfirst, width), bf16),
-            vmem((planes, piece - xfirst, width), bf16),
-            vmem((planes, xfirst, width), bf16),
+            vmem((planes, 2, xmost, width), bf16),
+            vmem((planes, 2, ymost, width), bf16),
+            vmem((planes, ymost, width), bf16),
+            vmem((planes, xmost, width), bf16),
             vmem((planes - 1, piece, width), bf16),
             vmem((seq, chans), f32),
             vmem((seq, chans), f32),
@@ -569,7 +595,7 @@
             vmem((planes, 2, rows, 2 * top), f32),
             dma((count,)),
             dma((count,)),
-            dma((12,)),
+            dma((17,)),
         ],
         compiler_params=pltpu.CompilerParams(
             collective_id=0, has_side_effects=True, vmem_limit_bytes=63 * 2**20

time: 96.4 us -> 92.9 us (0.964)
  Pallas kernels: 95.6 us -> 92.1 us
    pallas_call x1, Pallas kernels: 93.6 us -> 90.1 us  [fused(): pl.pallas_call(fused_kernel, out_shape=(jax.ShapeDtypeStruct((seq // lane...]
where the time goes in v2:
time: 92.9 us; the launch traced here: 92.8 us
  Pallas kernels  92.1 us (99%)
    pallas_call x1, Pallas kernels, fused(): pl.pallas_call(fused_kernel, out_shape=(jax.ShapeDtypeStruct((seq // lane...  90.1 us
    pallas_call x1, Pallas kernels, fused(): pl.pallas_call(hand_over, out_shape=tuple((jax.ShapeDtypeStruct(a.shape,...  2.02 us

profile of v2, /device:TPU:0, one launch (start us, length us, event | category | flops | bytes accessed | tf_op | source)
XLA Modules:
  0.0 92.8 jit_solution(7508205673364613616)
XLA Ops:
  0.6 90.1 %fused.1 = (bf16[128,2048]{1,0:T(8,128)(2,1)}, bf16[64,2048]{1,0:T(8,128)(2,1)}) custom-call(bf16[256,2048]{1,0:T(8,128)(2,1)} %tok_hbm.1, f32[1,2048]{1,0:T(1,128)} %bitcast.5, s32[4,256]{1,0:T(4,128)} %bitcast.6, f32[4,256]{1,0:T(4,128)} %bitcast.7, bf16[2,2048,256]{2,1,0:T(8,128)(2,1)} %wg_hbm.1, bf16[2,2048,256]{2,1,0:T(8,128)(2,1)} %wu_hbm.1, ...), custom_call_target="tpu_custom_call" | custom-call | flops 12884901888 | bytes 104857600 | tf_op jit(solution)/shard_map/fused/pallas_call | solution.py:549
  90.8 2.0 %hand_over.1 = (bf16[128,2048]{1,0:T(8,128)(2,1)}, bf16[64,2048]{1,0:T(8,128)(2,1)}) custom-call(bf16[128,2048]{1,0:T(8,128)(2,1)} %get-tuple-element.4.mixed, bf16[64,2048]{1,0:T(8,128)(2,1)} %get-tuple-element.5.routed), custom_call_target="tpu_custom_call" | custom-call | tf_op jit(solution)/shard_map/hand_over/pallas_call | solution.py:623
